TPU v7x, 32 devices: a whole 2x2x4 slice. The times are simulated.
32 devices in a mesh: grp: 2 (over x), ep: 16 (over z, y, core).
Axes of the slice: x: 2, y: 2, z: 4, core: 2. Of those that a mesh axis runs over, the one named last changes fastest.
Arguments:
- tokens: bfloat16 [1024, 2048], P(('grp', 'ep')), parts along dimension 0, may hold values from -6 to 6
- norm_gain: float32 [2048], replicated, may hold values from 0.5 to 4
- routes: int32 [1024, 4], P(('grp', 'ep')), parts along dimension 0, may hold values from 0 to 15, all different within a row; in each aligned block of 32 rows (0 to 31, 32 to 63, ...) at most 16 rows name the same one
- route_logits: float32 [1024, 4], P(('grp', 'ep')), parts along dimension 0, may hold values from -6 to 6
- w_gate: bfloat16 [16, 2048, 1792], P('ep'), may hold values from -0.125 to 0.125
- w_up: bfloat16 [16, 2048, 1792], P('ep'), may hold values from -0.125 to 0.125
- w_down: bfloat16 [16, 1792, 2048], P('ep'), may hold values from -0.125 to 0.125
Outputs:
- mixed: bfloat16 [1024, 2048], P(('grp', 'ep')), parts along dimension 0
There are 2 independent parts, one for each index of `grp`. A program takes and returns all parts, laid end to end along the dimension named above; an argument that names none is the same for every part. Nothing has to cross between parts.
Inputs may be any that keep to these rules, and one draw needn't show every extreme that they name: `routes`: each token names 4 different experts. Among the 32 tokens of one device no expert is named by more than 16 of them, and in every draw some expert is named by exactly 16 tokens of some device.
All inputs are finite; a program needn't handle non-finite values.
Results may differ from a plain program's by a relative error of at most 0.012.
Values may be sent and summed in bfloat16 or wider, within the bound.
A program may use at most 64 MiB of HBM per device.

v0:
```python
import jax
import jax.numpy as jnp
from jax import lax
from jax.sharding import PartitionSpec as P

TOP_K = 4


def rmsnorm(values, gain):
    floats = values.astype(jnp.float32)
    scaled = floats * lax.rsqrt(jnp.mean(floats * floats, axis=-1, keepdims=True) + 1e-06)
    return (scaled * gain).astype(jnp.bfloat16)


def expert(rows, gate_weight, up_weight, down_weight):
    gate = jnp.minimum(jnp.dot(rows, gate_weight, preferred_element_type=jnp.float32), 7.0)
    upper = jnp.clip(jnp.dot(rows, up_weight, preferred_element_type=jnp.float32), -7.0, 7.0)
    active = (gate * jax.nn.sigmoid(1.702 * gate) * (upper + 1.0)).astype(jnp.bfloat16)
    return jnp.dot(active, down_weight, preferred_element_type=jnp.float32).astype(jnp.bfloat16)


def shards(tokens, norm_gain, routes, route_logits, w_gate, w_up, w_down):
    tok_rows = tokens.shape[0]
    width = tokens.shape[1]
    n_experts = lax.axis_size("ep")
    capacity = max(2, 2 * tok_rows * TOP_K // n_experts)
    slot_count = n_experts * capacity
    normed = rmsnorm(tokens, norm_gain)
    route_weights = jax.nn.softmax(route_logits, axis=-1)
    slot_ids = jnp.arange(slot_count, dtype=jnp.int32)
    chosen = routes.reshape(-1)
    onehot = (chosen[:, None] == jnp.arange(n_experts, dtype=jnp.int32)[None, :]).astype(jnp.int32)
    within = jnp.sum(jnp.cumsum(onehot, axis=0) * onehot, axis=1) - 1
    slot_of = chosen * capacity + within
    placing = (slot_of[:, None] == slot_ids[None, :]).astype(jnp.bfloat16)
    repeated = jnp.repeat(normed, TOP_K, axis=0)
    outgoing = jnp.einsum("ps,pd->sd", placing, repeated, preferred_element_type=jnp.float32)
    outgoing = outgoing.astype(jnp.bfloat16).reshape(n_experts, capacity, width)
    arrived = lax.all_to_all(outgoing, "ep", split_axis=0, concat_axis=0, tiled=True)
    count = arrived.shape[1]
    rows_in = arrived.reshape(n_experts * count, width)
    result = expert(rows_in, w_gate[0], w_up[0], w_down[0]).reshape(n_experts, count, width)
    returned_rows = lax.all_to_all(result, "ep", split_axis=0, concat_axis=0, tiled=True)
    returned_rows = returned_rows.reshape(slot_count, width)
    picked = jnp.dot(placing, returned_rows, preferred_element_type=jnp.float32)
    total = jnp.sum(picked.reshape(tok_rows, TOP_K, width) * route_weights[:, :, None], axis=1)
    return total.astype(jnp.bfloat16)


def solution(mesh):
    in_specs = (
        P(("grp", "ep"), None),
        P(),
        P(("grp", "ep"), None),
        P(("grp", "ep"), None),
        P("ep", None, None),
        P("ep", None, None),
        P("ep", None, None),
    )
    out_specs = P(("grp", "ep"), None)
    return jax.shard_map(shards, mesh=mesh, in_specs=in_specs, out_specs=out_specs, check_vma=False)
```

profile of v0, /device:TPU:0, one launch (start us, length us, event | category | flops | bytes accessed | tf_op | source)
XLA Modules:
  0.0 81.3 jit_solution(8344682684116685522)
XLA Ops:
  0.0 0.8 copy.16
  0.8 0.1 eq.50
  0.9 0.1 fusion.38
  1.0 0.2 reduce_window_sum.11
  1.1 0.2 select_reduce_fusion
  1.3 1.0 %fusion.31 = f32[32]{0:T(128)S(1)} fusion(bf16[32,2048]{1,0:T(8,128)(2,1)} %param.7), kind=kLoop, calls=%fused_computation.21 | loop fusion | flops 196576 | bytes 131200 | tf_op jit(solution)/shard_map/reduce_sum | solution.py:11
  2.4 1.0 %fusion.33 = bf16[32,2048]{1,0:T(8,128)(2,1)S(1)} fusion(bf16[32,2048]{1,0:T(8,128)(2,1)} %param.7, f32[2048]{0:T(1024)} %param.8, f32[32]{0:T(128)S(1)} %add_rsqrt_fusion), kind=kLoop, calls=%fused_computation.23 | loop fusion | flops 262144 | bytes 270464 | tf_op jit(solution)/shard_map/convert_element_type | solution.py:12
  3.4 0.2 broadcast_in_dim.2
  3.6 0.1 reshape.65
  3.8 0.5 convolution_convert_fusion
  4.3 31.9 %all_to_all.10 = bf16[16,16,2048]{2,1,0:T(8,128)(2,1)S(1)} all-to-all(bf16[16,16,2048]{2,1,0:T(8,128)(2,1)S(1)} %bitcast.36), channel_id=1, replica_groups=mesh['grp'=2,'ep'=16] {'ep'}, dimensions={0} | all-to-all | bytes 2097152 | tf_op jit(solution)/shard_map/all_to_all | solution.py:39
  36.2 5.2 %fusion.9 = f32[256,1792]{1,0:T(8,128)S(1)} fusion(bf16[256,2048]{1,0:T(8,128)(2,1)S(1)} %bitcast.38, bf16[1,2048,1792]{2,1,0:T(8,128)(2,1)} %param.11), kind=kOutput, calls=%fused_computation.7 | convolution fusion | flops 1879506944 | bytes 10223616 | tf_op jit(solution)/shard_map/dot_general | solution.py:16
  41.4 10.8 %fusion.21 = bf16[256,2048]{1,0:T(8,128)(2,1)} fusion(bf16[1,1792,2048]{2,1,0:T(8,128)(2,1)} %param.13, bf16[256,2048]{1,0:T(8,128)(2,1)S(1)} %bitcast.39, bf16[1,2048,1792]{2,1,0:T(8,128)(2,1)} %param.12, f32[256,1792]{1,0:T(8,128)S(1)} %fusion.9), kind=kOutput, calls=%fused_computation.11 | convolution fusion | flops 3762749440 | bytes 18612224 | tf_op jit(solution)/shard_map/dot_general | solution.py:19
  52.2 0.0 copy-start
  52.2 0.0 copy-start.1
  52.2 5.2 %all-to-all-start.1 = ((bf16[16,16,2048]{2,1,0:T(8,128)(2,1)}), bf16[16,16,2048]{2,1,0:T(8,128)(2,1)S(1)}, u32[]{:S(2)}, u32[]{:S(2)}) async-start(bf16[16,16,2048]{2,1,0:T(8,128)(2,1)} %bitcast.6), calls=%async_computation.1 | async-start | bytes 2097152 | tf_op jit(solution)/shard_map/all_to_all | solution.py:43
  57.4 0.1 sub.15
  57.5 0.1 copy.17
  57.5 0.0 copy-done
  57.6 0.0 copy-done.1
  57.6 22.6 %all-to-all-done.1 = bf16[16,16,2048]{2,1,0:T(8,128)(2,1)S(1)} async-done(((bf16[16,16,2048]{2,1,0:T(8,128)(2,1)}), bf16[16,16,2048]{2,1,0:T(8,128)(2,1)S(1)}, u32[]{:S(2)}, u32[]{:S(2)}) %all-to-all-start.1) | async-done | bytes 1048608 | tf_op jit(solution)/shard_map/all_to_all | solution.py:43
  80.3 1.0 %fusion.24 = bf16[32,2048]{1,0:T(8,128)(2,1)} fusion(bf16[256,2048,1]{1,0,2:T(8,128)(2,1)S(1)} %bitcast.37, f32[32,4]{0,1:T(4,128)S(1)} %fusion.39, s32[32,4]{0,1:T(4,128)S(1)} %multiply_add_fusion), kind=kOutput, calls=%fused_computation.14 | convolution fusion | flops 134709248 | bytes 1180672 | tf_op jit(solution)/shard_map/dot_general | solution.py:45
  (6 shorter events, 0.1 us)
Async XLA Ops:
  52.2 5.3 %copy-start = (f32[32,4]{0,1:T(4,128)S(1)}, f32[32,4]{0,1:T(4,128)}, u32[]{:S(2)}) copy-start(f32[32,4]{0,1:T(4,128)} %param.10) | copy-start | bytes 1540
  52.2 5.4 %copy-start.1 = (s32[32,4]{0,1:T(4,128)S(1)}, s32[32,4]{0,1:T(4,128)}, u32[]{:S(2)}) copy-start(s32[32,4]{0,1:T(4,128)} %param.9) | copy-start | bytes 1540
  52.2 28.1 %all-to-all-start.1 = ((bf16[16,16,2048]{2,1,0:T(8,128)(2,1)}), bf16[16,16,2048]{2,1,0:T(8,128)(2,1)S(1)}, u32[]{:S(2)}, u32[]{:S(2)}) async-start(bf16[16,16,2048]{2,1,0:T(8,128)(2,1)} %bitcast.6), calls=%async_computation.1 | async-start | bytes 2097152 | tf_op jit(solution)/shard_map/all_to_all | solution.py:43
where the time goes:
time: 82.8 us; the launch traced here: 81.3 us
  blocking collectives  31.9 us (39%)
  waiting for transfers between devices  22.6 us (27%)
  matrix products  17.5 us (21%)
  starting transfers between devices  5.16 us (6%)
  other arithmetic  2.56 us (3%)
  local copies, waits for them, and re-layouts  1.39 us (2%)
    all_to_all x1, blocking collectives, shards(): lax.all_to_all(outgoing, 'ep', split_axis=0, concat_axis=0, tiled=True)  31.9 us
    all_to_all x1, waiting for transfers between devices, shards(): lax.all_to_all(result, 'ep', split_axis=0, concat_axis=0, tiled=True)  22.6 us
    dot_general x1, matrix products, expert(): jnp.dot(active, down_weight, preferred_element_type=jnp.float32)  10.8 us
    dot_general x1, matrix products, expert(): jnp.dot(rows, gate_weight, preferred_element_type=jnp.float32)  5.16 us
    all_to_all x1, starting transfers between devices, shards(): lax.all_to_all(result, 'ep', split_axis=0, concat_axis=0, tiled=True)  5.16 us
  transfers between devices with their start and end apart: 1, of which 1 were waited for; matrix products, arithmetic and copies ran while one was open for 0% of the time, Pallas kernels for 0%

commit v1 on v0

v1 whole, which is shorter than its diff:
```python
import functools

import jax
import jax.numpy as jnp
from jax import lax
from jax.experimental import pallas as pl
from jax.experimental.pallas import tpu as pltpu
from jax.sharding import PartitionSpec as P

TOP_K = 4
LANES = 128
TILE = 256
F32 = jnp.float32
BF16 = jnp.bfloat16


def flip(value, bits):
    out, bit = value, 1
    while bit <= bits:
        if bits & bit:
            out = out + bit - 2 * bit * ((value // bit) % 2)
        bit *= 2
    return out


def layer(n, cap, zs, ys, x_ref, gain_ref, meta_ref, wg_hbm, wu_hbm, wd_hbm, o_ref,
          wg, wu, wd, G, M, X, H, O, Psib, Pown, R1, Q, R2, T, R3, F4, R4,
          w_sem, m_send, m_recv, z_send, y_send, s_send, g_recv,
          r1_send, r1_recv, q_send, r2_recv, t_send, r3_recv, r4_send, r4_recv):
    me = lax.axis_index("ep")
    core = me % 2
    chip = me // 2
    z = chip // ys
    y = chip % ys
    sib = chip * 2 + 1 - core
    rows, width = x_ref.shape
    ff = wg.shape[1]
    half = width // 2
    chips = n // 2

    def dev(zz, yy, cc):
        return (zz * ys + yy) * 2 + cc

    def remote(src, dst, send, recv, target):
        return pltpu.make_async_remote_copy(
            src_ref=src, dst_ref=dst, send_sem=send, recv_sem=recv,
            device_id={"ep": target}, device_id_type=pl.DeviceIdType.MESH)

    loads = []
    for i, (src, dst) in enumerate(((wg_hbm, wg), (wu_hbm, wu), (wd_hbm, wd))):
        k = src.shape[1] // 2
        for h in range(2):
            c = pltpu.make_async_copy(src.at[0, pl.ds(h * k, k)], dst.at[pl.ds(h * k, k)], w_sem.at[i, h])
            c.start()
            loads.append(c)

    x = x_ref[...].astype(F32)
    normed = x * lax.rsqrt(jnp.mean(x * x, axis=-1, keepdims=True) + 1e-06) * gain_ref[...]
    G[me] = normed.astype(BF16)
    M[me] = meta_ref[...]

    barrier = pltpu.get_barrier_semaphore()
    for d in range(1, n):
        pl.semaphore_signal(barrier, inc=1, device_id={"ep": (me + d) % n},
                            device_id_type=pl.DeviceIdType.MESH)
    pl.semaphore_wait(barrier, n - 1)

    sends = []

    def go(copy):
        copy.start()
        sends.append(copy)

    def pass_on(src, send, target):
        go(remote(G.at[src], G.at[src], send, g_recv.at[src], target))

    def landed(src):
        remote(G.at[src], G.at[src], z_send.at[0], g_recv.at[src], sib).wait_recv()

    for d in range(1, n):
        go(remote(meta_ref, M.at[me], m_send.at[d], m_recv.at[me], (me + d) % n))
    for d in range(1, zs):
        pass_on(me, z_send.at[d], dev(flip(z, d), y, core))
    if ys > 1:
        pass_on(me, y_send.at[0], dev(z, 1 - y, core))
    pass_on(me, s_send.at[0], sib)
    for d in range(1, zs):
        src = dev(flip(z, d), y, core)
        landed(src)
        if ys > 1:
            pass_on(src, y_send.at[d], dev(z, 1 - y, core))
        pass_on(src, s_send.at[d], sib)

    for d in range(1, n):
        src = (me + n - d) % n
        remote(M.at[src], M.at[src], m_send.at[0], m_recv.at[src], sib).wait_recv()
    meta = M[...]
    hit = (meta[:, 0:TOP_K, :] == me.astype(F32)).astype(F32)
    sel = jnp.sum(hit, axis=1)
    weight = jnp.sum(hit * meta[:, TOP_K:2 * TOP_K, :], axis=1)
    before = lax.broadcasted_iota(jnp.int32, (LANES, LANES), 0) <= lax.broadcasted_iota(jnp.int32, (LANES, LANES), 1)
    rank = jnp.dot(sel.astype(BF16), before.astype(F32).astype(BF16), preferred_element_type=F32)
    key = jnp.where(sel > 0.0, rank - 1.0, -1.0)
    per = LANES // rows
    slots = per * cap
    picks, scales = [], []
    for q in range(n // per):
        own = key[q * per:(q + 1) * per]
        place = lax.broadcasted_iota(jnp.int32, (per, cap, LANES), 1).astype(F32)
        pick = (place == own[:, None, :]).astype(F32)
        scale = jnp.sum(pick * weight[q * per:(q + 1) * per][:, None, :], axis=2, keepdims=True)
        picks.append(pick.reshape(slots, LANES))
        scales.append(scale.reshape(slots, 1))
    scale = jnp.concatenate(scales, axis=0)

    if ys > 1:
        for d in range(zs):
            src = dev(flip(z, d), 1 - y, core)
            landed(src)
            pass_on(src, s_send.at[zs + d], sib)
    for d in range(zs):
        for yy in range(ys):
            landed(dev(flip(z, d), yy, 1 - core))

    for q in range(n // per):
        block = G[q * per:(q + 1) * per].reshape(LANES, width)
        X[q * slots:(q + 1) * slots, :] = jnp.dot(
            picks[q].astype(BF16), block, preferred_element_type=F32).astype(BF16)

    for c in loads[:4]:
        c.wait()

    @pl.loop(0, ff // TILE)
    def _(t):
        cols = pl.ds(pl.multiple_of(t * TILE, TILE), TILE)
        gate = jnp.minimum(jnp.dot(X[...], wg[:, cols], preferred_element_type=F32), 7.0)
        upper = jnp.clip(jnp.dot(X[...], wu[:, cols], preferred_element_type=F32), -7.0, 7.0)
        H[:, cols] = (gate * jax.nn.sigmoid(1.702 * gate) * (upper + 1.0)).astype(BF16)

    for c in loads[4:]:
        c.wait()

    def down(base, dst):
        @pl.loop(0, half // TILE)
        def _(t):
            cols = pl.ds(pl.multiple_of(base + t * TILE, TILE), TILE)
            here = pl.ds(pl.multiple_of(t * TILE, TILE), TILE)
            out = jnp.dot(H[...], wd[:, cols], preferred_element_type=F32)
            O[:, here] = (out * scale).astype(BF16)
        for q in range(n // per):
            spread = jnp.dot(picks[q].T.astype(BF16), O[q * slots:(q + 1) * slots, :],
                             preferred_element_type=F32).astype(BF16)
            dst[q * per:(q + 1) * per] = spread.reshape(per, rows, half)

    down((1 - core) * half, Psib)
    first = remote(Psib, R1, r1_send, r1_recv, sib)
    go(first)
    down(core * half, Pown)
    first.wait_recv()

    def pair(zz, yy):
        at = pl.ds(dev(zz, yy, 0), 2)
        return Pown[at].astype(F32) + R1[at].astype(F32)

    order = list(range(zs - 1, -1, -1))
    if ys > 1:
        for d in order:
            Q[d] = pair(flip(z, d), 1 - y).astype(BF16)
            go(remote(Q.at[d], R2.at[d], q_send.at[d], r2_recv.at[d], dev(z, 1 - y, core)))
    final = None
    for d in order:
        total = pair(flip(z, d), y)
        if ys > 1:
            remote(Q.at[d], R2.at[d], q_send.at[d], r2_recv.at[d], sib).wait_recv()
            total = total + R2[d].astype(F32)
        if d:
            T[d] = total.astype(BF16)
            go(remote(T.at[d], R3.at[d], t_send.at[d], r3_recv.at[d], dev(flip(z, d), y, core)))
        else:
            final = total
    for d in order[:-1]:
        remote(T.at[d], R3.at[d], t_send.at[d], r3_recv.at[d], sib).wait_recv()
        final = final + R3[d].astype(F32)
    F4[...] = final.astype(BF16)
    last = remote(F4.at[1 - core], R4, r4_send, r4_recv, sib)
    go(last)
    mine = pl.ds(pl.multiple_of(core * half, half), half)
    other = pl.ds(pl.multiple_of((1 - core) * half, half), half)
    o_ref[:, mine] = F4[core]
    last.wait_recv()
    o_ref[:, other] = R4[...]
    for copy in sends:
        copy.wait_send()


def shards(n, tokens, norm_gain, routes, route_logits, w_gate, w_up, w_down):
    rows, width = tokens.shape
    ff = w_gate.shape[2]
    cap = max(2, 2 * rows * TOP_K // n)
    chips = n // 2
    ys = 2 if chips <= 8 else 1
    zs = chips // ys
    per = LANES // rows
    me = lax.axis_index("ep")
    here = (jnp.arange(LANES) // rows == me % per)[None, :]
    chosen = jnp.where(here, jnp.tile(routes.astype(F32).T, (1, per)), -1.0)
    weights = jnp.where(here, jnp.tile(jax.nn.softmax(route_logits, axis=-1).T, (1, per)), 0.0)
    meta = jnp.concatenate([chosen, weights], axis=0)
    vmem = pl.BlockSpec(memory_space=pltpu.VMEM)
    hbm = pl.BlockSpec(memory_space=pl.ANY)
    half = width // 2
    dma = pltpu.SemaphoreType.DMA
    return pl.pallas_call(
        functools.partial(layer, n, cap, zs, ys),
        out_shape=jax.ShapeDtypeStruct((rows, width), BF16),
        in_specs=[vmem, vmem, vmem, hbm, hbm, hbm],
        out_specs=vmem,
        scratch_shapes=[
            pltpu.VMEM((width, ff), BF16),
            pltpu.VMEM((width, ff), BF16),
            pltpu.VMEM((ff, width), BF16),
            pltpu.VMEM((n, rows, width), BF16),
            pltpu.VMEM((n, 2 * TOP_K, LANES), F32),
            pltpu.VMEM((n * cap, width), BF16),
            pltpu.VMEM((n * cap, ff), BF16),
            pltpu.VMEM((n * cap, half), BF16),
            pltpu.VMEM((n, rows, half), BF16),
            pltpu.VMEM((n, rows, half), BF16),
            pltpu.VMEM((n, rows, half), BF16),
            pltpu.VMEM((zs, 2, rows, half), BF16),
            pltpu.VMEM((zs, 2, rows, half), BF16),
            pltpu.VMEM((zs, 2, rows, half), BF16),
            pltpu.VMEM((zs, 2, rows, half), BF16),
            pltpu.VMEM((2, rows, half), BF16),
            pltpu.VMEM((rows, half), BF16),
            dma((3, 2)), dma((n,)), dma((n,)), dma((zs,)), dma((zs,)), dma((chips,)), dma((n,)),
            dma, dma, dma((zs,)), dma((zs,)), dma((zs,)), dma((zs,)), dma, dma,
        ],
        compiler_params=pltpu.CompilerParams(
            collective_id=0, has_side_effects=True, vmem_limit_bytes=60 * 1024 * 1024),
    )(tokens, norm_gain.reshape(1, width), meta, w_gate, w_up, w_down)


def solution(mesh):
    in_specs = (
        P(("grp", "ep"), None),
        P(),
        P(("grp", "ep"), None),
        P(("grp", "ep"), None),
        P("ep", None, None),
        P("ep", None, None),
        P("ep", None, None),
    )
    out_specs = P(("grp", "ep"), None)
    body = functools.partial(shards, mesh.shape["ep"])
    return jax.shard_map(body, mesh=mesh, in_specs=in_specs, out_specs=out_specs, check_vma=False)
```

time: 82.8 us -> 62.3 us (0.75); the launches traced: 81.3 us -> 62.1 us
  Pallas kernels: 0 us -> 56.9 us
  blocking collectives: 31.9 us -> 0 us
  waiting for transfers between devices: 22.6 us -> 0 us
  matrix products: 17.5 us -> 0 us
  starting transfers between devices: 5.16 us -> 0 us
  other arithmetic: 2.56 us -> 3.4 us
    pallas_call x0 -> x1, Pallas kernels: none -> 56.9 us  [shards(): pl.pallas_call(functools.partial(layer, n, cap, zs, ys), out_shape=jax.Sh...]
    all_to_all x1 -> x0, blocking collectives: 31.9 us -> none  [shards(): lax.all_to_all(outgoing, 'ep', split_axis=0, concat_axis=0, tiled=True)]
    all_to_all x1 -> x0, waiting for transfers between devices: 22.6 us -> none  [shards(): lax.all_to_all(result, 'ep', split_axis=0, concat_axis=0, tiled=True)]
    dot_general x4 -> x0, matrix products: 17.5 us -> none  [the longest x1 10.8 us: expert(): jnp.dot(active, down_weight, preferred_element_type=jnp.float32)]
    all_to_all x1 -> x0, starting transfers between devices: 5.16 us -> none  [shards(): lax.all_to_all(result, 'ep', split_axis=0, concat_axis=0, tiled=True)]
    transpose x0 -> x2, other arithmetic: none -> 1.38 us  [the longest x1 0.69 us: shards(): jax.nn.softmax(route_logits, axis=-1)]
    convert_element_type x2 -> x0, other arithmetic: 1.1 us -> none  [the longest x1 1.01 us: rmsnorm(): return (scaled * gain).astype(jnp.bfloat16)]
  transfers between devices with their start and end apart: 1 -> 0, of which waited for: 1 -> 0; matrix products, arithmetic and copies ran while one was open for 0% -> 0% of each run, Pallas kernels for 0% -> 0%
where the time goes in v1:
time: 62.3 us; the launch traced here: 62.1 us
  Pallas kernels  56.9 us (91%)
  other arithmetic  3.4 us (5%)
  local copies, waits for them, and re-layouts  1.75 us (3%)
    pallas_call x1, Pallas kernels, shards(): pl.pallas_call(functools.partial(layer, n, cap, zs, ys), out_shape=jax.Sh...  56.9 us
    unnamed x1, local copies, waits for them, and re-layouts  1.57 us

profile of v1, /device:TPU:0, one launch (start us, length us, event | category | flops | bytes accessed | tf_op | source)
XLA Modules:
  0.0 62.1 jit_solution(6702092958418681226)
XLA Ops:
  0.0 0.7 %reduce_max.9 = f32[32]{0:T(128)S(1)} reduce(f32[32,4]{0,1:T(4,128)} %param.10, f32[]{:T(128)} %constant.39.clone.1), dimensions={1}, to_apply=%region_0.1 | reduce | flops 96 | bytes 644 | tf_op jit(solution)/shard_map/reduce_max | solution.py:207
  0.7 0.7 %fusion = f32[32]{0:T(128)S(1)} fusion(f32[32,4]{0,1:T(4,128)} %param.10, f32[32]{0:T(128)S(1)} %reduce_max.9), kind=kLoop, calls=%fused_computation.5 | loop fusion | flops 224 | bytes 768 | tf_op jit(solution)/shard_map/reduce_sum | solution.py:207
  1.4 0.7 %divide_bitcast_fusion = f32[4,32]{1,0:T(4,128)S(1)} fusion(f32[32,4]{0,1:T(4,128)} %param.10, f32[32]{0:T(128)S(1)} %fusion, f32[32]{0:T(128)S(1)} %reduce_max.9), kind=kLoop, calls=%fused_computation.1 | loop fusion | flops 256 | bytes 1280 | tf_op jit(solution)/shard_map/transpose | solution.py:207
  2.1 0.7 %convert_bitcast_fusion = f32[4,32]{1,0:T(4,128)S(1)} fusion(s32[32,4]{0,1:T(4,128)} %param.9), kind=kLoop, calls=%fused_computation.3 | loop fusion | flops 128 | bytes 1024 | tf_op jit(solution)/shard_map/transpose | solution.py:206
  2.8 0.1 tile.9
  2.9 0.1 tile.21
  3.0 0.6 pad_maximum_fusion.meta_ref
  3.6 56.9 %shard_map.73 = bf16[32,2048]{1,0:T(8,128)(2,1)} custom-call(bf16[32,2048]{1,0:T(8,128)(2,1)} %x_ref.1, f32[1,2048]{1,0:T(1,128)} %bitcast.5, f32[8,128]{1,0:T(8,128)} %pad_maximum_fusion.meta_ref, bf16[1,2048,1792]{2,1,0:T(8,128)(2,1)} %wg_hbm.1, bf16[1,2048,1792]{2,1,0:T(8,128)(2,1)} %wu_hbm.1, bf16[1,1792,2048]{2,1,0:T(8,128)(2,1)} %wd_hbm.1), custom_call_target="tpu_custom_call" | custom-call | tf_op jit(solution)/shard_map/pallas_call | solution.py:213
  60.5 1.6 %copy.9 = bf16[32,2048]{1,0:T(8,128)(2,1)} copy(bf16[32,2048]{1,0:T(8,128)(2,1)} %shard_map.73) | data formatting | bytes 262144
  (4 shorter events, 0.0 us)

commit v2 on v1

v2 whole, which is shorter than its diff:
```python
import functools

import jax
import jax.numpy as jnp
from jax import lax
from jax.experimental import pallas as pl
from jax.experimental.pallas import tpu as pltpu
from jax.sharding import PartitionSpec as P

TOP_K = 4
LANES = 128
TILE = 256
PARTS = 2
F32 = jnp.float32
BF16 = jnp.bfloat16


def layer(n, cap, zs, ys, x_ref, gain_ref, routes_ref, logits_ref, wg_hbm, wu_hbm, wd_hbm, o_ref,
          wg, wu, wd, G, M, X, H, O, Psib, Pown, R1, Q, R2, T, RZ, acc, F4, R4,
          w_sem, m_send, m_recv, z_send, y_send, s_send, g_recv,
          r1_send, r1_recv, q_send, r2_recv, t_send, rz_recv, r4_send, r4_recv):
    me = lax.axis_index("ep")
    core = me % 2
    chip = me // 2
    z = chip // ys
    y = chip % ys
    sib = chip * 2 + 1 - core
    rows, width = x_ref.shape
    ff = wg.shape[1]
    half = width // 2
    part = half // PARTS
    per = LANES // rows
    slots = per * cap

    def dev(zz, yy, cc):
        return (zz * ys + yy) * 2 + cc

    def remote(src, dst, send, recv, target):
        return pltpu.make_async_remote_copy(
            src_ref=src, dst_ref=dst, send_sem=send, recv_sem=recv,
            device_id={"ep": target}, device_id_type=pl.DeviceIdType.MESH)

    steps = []
    for k in range(1, zs):
        steps.append((2 * k - 1, -k, z >= k))
        steps.append((2 * k, k, z < zs - k))

    loads = []
    for i, (src, dst) in enumerate(((wg_hbm, wg), (wu_hbm, wu), (wd_hbm, wd))):
        k = src.shape[1] // 2
        for h in range(2):
            c = pltpu.make_async_copy(src.at[0, pl.ds(h * k, k)], dst.at[pl.ds(h * k, k)], w_sem.at[i, h])
            c.start()
            loads.append(c)

    x = x_ref[...].astype(F32)
    normed = x * lax.rsqrt(jnp.mean(x * x, axis=-1, keepdims=True) + 1e-06) * gain_ref[...]
    G[me] = normed.astype(BF16)
    spot = (lax.broadcasted_iota(jnp.int32, (rows, LANES), 0) + rows * (me % per)
            == lax.broadcasted_iota(jnp.int32, (rows, LANES), 1)).astype(F32)

    def turned(values):
        return lax.dot_general(values, spot, (((0,), (0,)), ((), ())),
                               precision=lax.Precision.HIGHEST, preferred_element_type=F32)

    logits = logits_ref[...]
    powers = jnp.exp(logits - jnp.max(logits, axis=-1, keepdims=True))
    M[me, 0:TOP_K] = turned((routes_ref[...] + 1).astype(F32))
    M[me, TOP_K:2 * TOP_K] = turned(powers / jnp.sum(powers, axis=-1, keepdims=True))

    barrier = pltpu.get_barrier_semaphore()
    for d in range(1, n):
        pl.semaphore_signal(barrier, inc=1, device_id={"ep": (me + d) % n},
                            device_id_type=pl.DeviceIdType.MESH)
    pl.semaphore_wait(barrier, n - 1)

    sends = []

    def go(copy, there=None):
        if there is None:
            copy.start()
        else:
            pl.when(there)(copy.start)
        sends.append((copy, there))

    def pass_on(src, send, target, there=None):
        go(remote(G.at[src], G.at[src], send, g_recv.at[src], target), there)

    def landed(src):
        remote(G.at[src], G.at[src], z_send.at[0], g_recv.at[src], sib).wait_recv()

    up, down_there = z < zs - 1, z >= 1
    pass_on(me, z_send.at[0], dev(z + 1, y, core), up)
    pass_on(me, z_send.at[2 * zs], dev(z - 1, y, core), down_there)
    if ys > 1:
        pass_on(me, y_send.at[0], dev(z, 1 - y, core))
    pass_on(me, s_send.at[0], sib)
    for d in range(1, n):
        go(remote(M.at[me], M.at[me], m_send.at[d], m_recv.at[me], (me + d) % n))

    for i, k, there in steps:
        src = dev(z + k, y, core)
        pl.when(there)(functools.partial(landed, src))
        if k < 0:
            pass_on(src, z_send.at[i], dev(z + 1, y, core), there & up)
        else:
            pass_on(src, z_send.at[i], dev(z - 1, y, core), there & down_there)
        if ys > 1:
            pass_on(src, y_send.at[i], dev(z, 1 - y, core), there)
        pass_on(src, s_send.at[i], sib, there)

    for d in range(1, n):
        src = (me + n - d) % n
        remote(M.at[src], M.at[src], m_send.at[0], m_recv.at[src], sib).wait_recv()
    meta = M[...]
    hit = (meta[:, 0:TOP_K, :] == (me + 1).astype(F32)).astype(F32)
    sel = jnp.sum(hit, axis=1)
    weight = jnp.sum(hit * meta[:, TOP_K:2 * TOP_K, :], axis=1)
    before = lax.broadcasted_iota(jnp.int32, (LANES, LANES), 0) <= lax.broadcasted_iota(jnp.int32, (LANES, LANES), 1)
    rank = jnp.dot(sel.astype(BF16), before.astype(F32).astype(BF16), preferred_element_type=F32)
    key = jnp.where(sel > 0.0, rank - 1.0, -1.0)
    picks, scales = [], []
    for q in range(n // per):
        own = key[q * per:(q + 1) * per]
        place = lax.broadcasted_iota(jnp.int32, (per, cap, LANES), 1).astype(F32)
        pick = (place == own[:, None, :]).astype(F32)
        scale = jnp.sum(pick * weight[q * per:(q + 1) * per][:, None, :], axis=2, keepdims=True)
        picks.append(pick.reshape(slots, LANES))
        scales.append(scale.reshape(slots, 1))
    scale = jnp.concatenate(scales, axis=0)

    if ys > 1:
        landed(dev(z, 1 - y, core))
        pass_on(dev(z, 1 - y, core), s_send.at[2 * zs], sib)
        for i, k, there in steps:
            src = dev(z + k, 1 - y, core)
            pl.when(there)(functools.partial(landed, src))
            pass_on(src, s_send.at[2 * zs + i], sib, there)
    for yy in range(ys):
        landed(dev(z, yy, 1 - core))
        for i, k, there in steps:
            pl.when(there)(functools.partial(landed, dev(z + k, yy, 1 - core)))

    for q in range(n // per):
        block = G[q * per:(q + 1) * per].reshape(LANES, width)
        X[q * slots:(q + 1) * slots, :] = jnp.dot(
            picks[q].astype(BF16), block, preferred_element_type=F32).astype(BF16)

    for c in loads[:4]:
        c.wait()

    @pl.loop(0, ff // TILE)
    def _(t):
        cols = pl.ds(pl.multiple_of(t * TILE, TILE), TILE)
        gate = jnp.minimum(jnp.dot(X[...], wg[:, cols], preferred_element_type=F32), 7.0)
        upper = jnp.clip(jnp.dot(X[...], wu[:, cols], preferred_element_type=F32), -7.0, 7.0)
        H[:, cols] = (gate * jax.nn.sigmoid(1.702 * gate) * (upper + 1.0)).astype(BF16)

    for c in loads[4:]:
        c.wait()

    def down(base, dst):
        @pl.loop(0, part // TILE)
        def _(t):
            cols = pl.ds(pl.multiple_of(base + t * TILE, TILE), TILE)
            here = pl.ds(pl.multiple_of(t * TILE, TILE), TILE)
            out = jnp.dot(H[...], wd[:, cols], preferred_element_type=F32)
            O[:, here] = (out * scale).astype(BF16)
        for q in range(n // per):
            spread = jnp.dot(picks[q].T.astype(BF16), O[q * slots:(q + 1) * slots, :],
                             preferred_element_type=F32).astype(BF16)
            dst[q * per:(q + 1) * per] = spread.reshape(per, rows, part)

    def pair(p, zz, yy):
        at = pl.ds(dev(zz, yy, 0), 2)
        return Pown[p, at].astype(F32) + R1[p, at].astype(F32)

    far = steps[::-1]

    def to_core(p):
        down((1 - core) * half + p * part, Psib.at[p])
        go(remote(Psib.at[p], R1.at[p], r1_send.at[p], r1_recv.at[p], sib))

    def to_y(p):
        remote(Psib.at[p], R1.at[p], r1_send.at[p], r1_recv.at[p], sib).wait_recv()
        if ys > 1:
            for i, k, there in far + [(0, 0, None)]:
                def put(i=i, k=k):
                    Q[p, i] = pair(p, z + k, 1 - y).astype(BF16)
                if there is None:
                    put()
                else:
                    pl.when(there)(put)
                go(remote(Q.at[p, i], R2.at[p, i], q_send.at[p, i], r2_recv.at[p, i], dev(z, 1 - y, core)), there)

    def gathered(p, i, k):
        total = pair(p, z + k, y)
        if ys > 1:
            remote(Q.at[p, i], R2.at[p, i], q_send.at[p, i], r2_recv.at[p, i], sib).wait_recv()
            total = total + R2[p, i].astype(F32)
        return total

    def take(p, i):
        remote(T.at[p, i], RZ.at[p, i], t_send.at[p, i], rz_recv.at[p, i], sib).wait_recv()
        acc[...] += RZ[p, i].astype(F32)

    def to_z(p):
        for i, k, there in far:
            def put(i=i, k=k):
                acc[...] = gathered(p, i, k)
                if k > 0 and k < zs - 1:
                    pl.when(down_there)(functools.partial(take, p, i + 2))
                if k < 0 and k > 1 - zs:
                    pl.when(up)(functools.partial(take, p, i + 2))
                T[p, i] = acc[...].astype(BF16)
            pl.when(there)(put)
            target = dev(z + 1, y, core) if k > 0 else dev(z - 1, y, core)
            go(remote(T.at[p, i], RZ.at[p, i], t_send.at[p, i], rz_recv.at[p, i], target), there)

    def to_end(p):
        acc[...] = gathered(p, 0, 0)
        if zs > 1:
            pl.when(down_there)(functools.partial(take, p, 2))
            pl.when(up)(functools.partial(take, p, 1))
        F4[p] = acc[...].astype(BF16)
        go(remote(F4.at[p, 1 - core], R4.at[p], r4_send.at[p], r4_recv.at[p], sib))

    to_core(0)
    down(core * half, Pown.at[0])
    for p in range(1, PARTS):
        to_core(p)
        to_y(p - 1)
        down(core * half + p * part, Pown.at[p])
    to_y(PARTS - 1)
    to_z(0)
    for p in range(1, PARTS):
        to_z(p)
    for p in range(PARTS):
        to_end(p)
    for p in range(PARTS):
        o_ref[:, pl.ds(pl.multiple_of(core * half + p * part, part), part)] = F4[p, core]
    for p in range(PARTS):
        remote(F4.at[p, 1 - core], R4.at[p], r4_send.at[p], r4_recv.at[p], sib).wait_recv()
        o_ref[:, pl.ds(pl.multiple_of((1 - core) * half + p * part, part), part)] = R4[p]
    for copy, there in sends:
        if there is None:
            copy.wait_send()
        else:
            pl.when(there)(copy.wait_send)


def shards(n, tokens, norm_gain, routes, route_logits, w_gate, w_up, w_down):
    rows, width = tokens.shape
    ff = w_gate.shape[2]
    cap = max(2, 2 * rows * TOP_K // n)
    chips = n // 2
    ys = 2 if chips <= 8 else 1
    zs = chips // ys
    vmem = pl.BlockSpec(memory_space=pltpu.VMEM)
    hbm = pl.BlockSpec(memory_space=pl.ANY)
    part = width // 2 // PARTS
    dma = pltpu.SemaphoreType.DMA
    side = pltpu.VMEM((PARTS, n, rows, part), BF16)
    line = pltpu.VMEM((PARTS, 2 * zs - 1, 2, rows, part), BF16)
    return pl.pallas_call(
        functools.partial(layer, n, cap, zs, ys),
        out_shape=jax.ShapeDtypeStruct((rows, width), BF16),
        in_specs=[vmem, vmem, vmem, vmem, hbm, hbm, hbm],
        out_specs=vmem,
        scratch_shapes=[
            pltpu.VMEM((width, ff), BF16),
            pltpu.VMEM((width, ff), BF16),
            pltpu.VMEM((ff, width), BF16),
            pltpu.VMEM((n, rows, width), BF16),
            pltpu.VMEM((n, 2 * TOP_K, LANES), F32),
            pltpu.VMEM((n * cap, width), BF16),
            pltpu.VMEM((n * cap, ff), BF16),
            pltpu.VMEM((n * cap, part), BF16),
            side, side, side, line, line, line, line,
            pltpu.VMEM((2, rows, part), F32),
            pltpu.VMEM((PARTS, 2, rows, part), BF16),
            pltpu.VMEM((PARTS, rows, part), BF16),
            dma((3, 2)), dma((n,)), dma((n,)), dma((2 * zs + 1,)), dma((2 * zs,)), dma((4 * zs,)), dma((n,)),
            dma((PARTS,)), dma((PARTS,)), dma((PARTS, 2 * zs)), dma((PARTS, 2 * zs)),
            dma((PARTS, 2 * zs)), dma((PARTS, 2 * zs)), dma((PARTS,)), dma((PARTS,)),
        ],
        compiler_params=pltpu.CompilerParams(
            collective_id=0, has_side_effects=True, vmem_limit_bytes=60 * 1024 * 1024),
    )(tokens, norm_gain.reshape(1, width), routes, route_logits, w_gate, w_up, w_down)


def solution(mesh):
    in_specs = (
        P(("grp", "ep"), None),
        P(),
        P(("grp", "ep"), None),
        P(("grp", "ep"), None),
        P("ep", None, None),
        P("ep", None, None),
        P("ep", None, None),
    )
    out_specs = P(("grp", "ep"), None)
    body = functools.partial(shards, mesh.shape["ep"])
    return jax.shard_map(body, mesh=mesh, in_specs=in_specs, out_specs=out_specs, check_vma=False)
```

time: 62.3 us -> 61.1 us (0.981)
  other arithmetic: 3.4 us -> 0 us
  local copies, waits for them, and re-layouts: 1.75 us -> 4.29 us
    unnamed x1 -> x3, local copies, waits for them, and re-layouts: 1.57 us -> 4.29 us
    transpose x2 -> x0, other arithmetic: 1.38 us -> none  [the longest x1 0.69 us: shards(): jax.nn.softmax(route_logits, axis=-1)]
    reduce_sum x1 -> x0, other arithmetic: 0.7 us -> none  [shards(): jax.nn.softmax(route_logits, axis=-1)]
    reduce_max x1 -> x0, other arithmetic: 0.7 us -> none  [shards(): jax.nn.softmax(route_logits, axis=-1)]
where the time goes in v2:
time: 61.1 us; the launch traced here: 60.9 us
  Pallas kernels  56.6 us (93%)
  local copies, waits for them, and re-layouts  4.29 us (7%)
    pallas_call x1, Pallas kernels, shards(): pl.pallas_call(functools.partial(layer, n, cap, zs, ys), out_shape=jax.Sh...  56.6 us
    unnamed x3, local copies, waits for them, and re-layouts  4.29 us

profile of v2, /device:TPU:0, one launch (start us, length us, event | category | flops | bytes accessed | tf_op | source)
XLA Modules:
  0.0 60.9 jit_solution(12196004880869193068)
XLA Ops:
  0.0 1.4 %copy.8.routes_ref = s32[32,4]{1,0:T(8,128)} copy(s32[32,4]{0,1:T(4,128)} %param.9) | data formatting | bytes 1024 | tf_op args[2]
  1.4 1.4 %copy.9.logits_ref = f32[32,4]{1,0:T(8,128)} copy(f32[32,4]{0,1:T(4,128)} %param.10) | data formatting | bytes 1024 | tf_op args[3]
  2.7 56.6 %shard_map.73 = bf16[32,2048]{1,0:T(8,128)(2,1)} custom-call(bf16[32,2048]{1,0:T(8,128)(2,1)} %x_ref.1, f32[1,2048]{1,0:T(1,128)} %bitcast.1, s32[32,4]{1,0:T(8,128)} %copy.8.routes_ref, f32[32,4]{1,0:T(8,128)} %copy.9.logits_ref, bf16[1,2048,1792]{2,1,0:T(8,128)(2,1)} %wg_hbm.1, bf16[1,2048,1792]{2,1,0:T(8,128)(2,1)} %wu_hbm.1, bf16[1,1792,2048]{2,1,0:T(8,128)(2,1)} %wd_hbm.1), custom_call_target="tpu_custom_call" | custom-call | tf_op jit(solution)/shard_map/pallas_call | solution.py:265
  59.4 1.6 %copy.11 = bf16[32,2048]{1,0:T(8,128)(2,1)} copy(bf16[32,2048]{1,0:T(8,128)(2,1)} %shard_map.73) | data formatting | bytes 262144

commit v3 on v2

--- a/solution.py
+++ b/solution.py
@@ -11,6 +11,7 @@
 LANES = 128
 TILE = 256
 PARTS = 2
+SPLIT = 2
 F32 = jnp.float32
 BF16 = jnp.bfloat16
 
@@ -59,14 +60,13 @@
     spot = (lax.broadcasted_iota(jnp.int32, (rows, LANES), 0) + rows * (me % per)
             == lax.broadcasted_iota(jnp.int32, (rows, LANES), 1)).astype(F32)
 
-    def turned(values):
-        return lax.dot_general(values, spot, (((0,), (0,)), ((), ())),
-                               precision=lax.Precision.HIGHEST, preferred_element_type=F32)
+    def placed(values):
+        return jnp.dot(values, spot, precision=lax.Precision.HIGHEST, preferred_element_type=F32)
 
     logits = logits_ref[...]
-    powers = jnp.exp(logits - jnp.max(logits, axis=-1, keepdims=True))
-    M[me, 0:TOP_K] = turned((routes_ref[...] + 1).astype(F32))
-    M[me, TOP_K:2 * TOP_K] = turned(powers / jnp.sum(powers, axis=-1, keepdims=True))
+    powers = jnp.exp(logits - jnp.max(logits, axis=0, keepdims=True))
+    M[me, 0:TOP_K] = placed((routes_ref[...] + 1).astype(F32))
+    M[me, TOP_K:2 * TOP_K] = placed(powers / jnp.sum(powers, axis=0, keepdims=True))
 
     barrier = pltpu.get_barrier_semaphore()
     for d in range(1, n):
@@ -83,31 +83,53 @@
             pl.when(there)(copy.start)
         sends.append((copy, there))
 
-    def pass_on(src, send, target, there=None):
-        go(remote(G.at[src], G.at[src], send, g_recv.at[src], target), there)
-
-    def landed(src):
-        remote(G.at[src], G.at[src], z_send.at[0], g_recv.at[src], sib).wait_recv()
+    def piece(src, h):
+        return G.at[src, pl.ds(h * (rows // SPLIT), rows // SPLIT)]
+
+    def pass_on(src, h, send, i, target, there=None):
+        go(remote(piece(src, h), piece(src, h), send.at[i, h], g_recv.at[src, h], target), there)
+
+    def landed(src, h):
+        remote(piece(src, h), piece(src, h), z_send.at[0, h], g_recv.at[src, h], sib).wait_recv()
 
     up, down_there = z < zs - 1, z >= 1
-    pass_on(me, z_send.at[0], dev(z + 1, y, core), up)
-    pass_on(me, z_send.at[2 * zs], dev(z - 1, y, core), down_there)
-    if ys > 1:
-        pass_on(me, y_send.at[0], dev(z, 1 - y, core))
-    pass_on(me, s_send.at[0], sib)
+    for h in range(SPLIT):
+        pass_on(me, h, z_send, 0, dev(z + 1, y, core), up)
+        pass_on(me, h, z_send, 2 * zs, dev(z - 1, y, core), down_there)
+        if ys > 1:
+            pass_on(me, h, y_send, 0, dev(z, 1 - y, core))
+        pass_on(me, h, s_send, 0, sib)
     for d in range(1, n):
         go(remote(M.at[me], M.at[me], m_send.at[d], m_recv.at[me], (me + d) % n))
 
-    for i, k, there in steps:
+    def from_z(i, k, there):
         src = dev(z + k, y, core)
-        pl.when(there)(functools.partial(landed, src))
-        if k < 0:
-            pass_on(src, z_send.at[i], dev(z + 1, y, core), there & up)
-        else:
-            pass_on(src, z_send.at[i], dev(z - 1, y, core), there & down_there)
+        for h in range(SPLIT):
+            pl.when(there)(functools.partial(landed, src, h))
+            if k < 0:
+                pass_on(src, h, z_send, i, dev(z + 1, y, core), there & up)
+            else:
+                pass_on(src, h, z_send, i, dev(z - 1, y, core), there & down_there)
+            if ys > 1:
+                pass_on(src, h, y_send, i, dev(z, 1 - y, core), there)
+            pass_on(src, h, s_send, i, sib, there)
+
+    def from_y(i, k, there):
+        src = dev(z + k, 1 - y, core)
+        for h in range(SPLIT):
+            if there is None:
+                landed(src, h)
+            else:
+                pl.when(there)(functools.partial(landed, src, h))
+            pass_on(src, h, s_send, 2 * zs + i, sib, there)
+
+    late = [(0, 0, None)] + steps
+    for j in range(0, len(steps), 2):
+        for step in steps[j:j + 2]:
+            from_z(*step)
         if ys > 1:
-            pass_on(src, y_send.at[i], dev(z, 1 - y, core), there)
-        pass_on(src, s_send.at[i], sib, there)
+            for step in late[max(0, j - 1):j + 1]:
+                from_y(*step)
 
     for d in range(1, n):
         src = (me + n - d) % n
@@ -130,16 +152,13 @@
     scale = jnp.concatenate(scales, axis=0)
 
     if ys > 1:
-        landed(dev(z, 1 - y, core))
-        pass_on(dev(z, 1 - y, core), s_send.at[2 * zs], sib)
-        for i, k, there in steps:
-            src = dev(z + k, 1 - y, core)
-            pl.when(there)(functools.partial(landed, src))
-            pass_on(src, s_send.at[2 * zs + i], sib, there)
+        for step in late[max(0, len(steps) - 1):]:
+            from_y(*step)
     for yy in range(ys):
-        landed(dev(z, yy, 1 - core))
-        for i, k, there in steps:
-            pl.when(there)(functools.partial(landed, dev(z + k, yy, 1 - core)))
+        for h in range(SPLIT):
+            landed(dev(z, yy, 1 - core), h)
+            for i, k, there in steps:
+                pl.when(there)(functools.partial(landed, dev(z + k, yy, 1 - core), h))
 
     for q in range(n // per):
         block = G[q * per:(q + 1) * per].reshape(LANES, width)
@@ -280,13 +299,14 @@
             pltpu.VMEM((2, rows, part), F32),
             pltpu.VMEM((PARTS, 2, rows, part), BF16),
             pltpu.VMEM((PARTS, rows, part), BF16),
-            dma((3, 2)), dma((n,)), dma((n,)), dma((2 * zs + 1,)), dma((2 * zs,)), dma((4 * zs,)), dma((n,)),
+            dma((3, 2)), dma((n,)), dma((n,)), dma((2 * zs + 1, SPLIT)), dma((2 * zs, SPLIT)), dma((4 * zs, SPLIT)),
+            dma((n, SPLIT)),
             dma((PARTS,)), dma((PARTS,)), dma((PARTS, 2 * zs)), dma((PARTS, 2 * zs)),
             dma((PARTS, 2 * zs)), dma((PARTS, 2 * zs)), dma((PARTS,)), dma((PARTS,)),
         ],
         compiler_params=pltpu.CompilerParams(
             collective_id=0, has_side_effects=True, vmem_limit_bytes=60 * 1024 * 1024),
-    )(tokens, norm_gain.reshape(1, width), routes, route_logits, w_gate, w_up, w_down)
+    )(tokens, norm_gain.reshape(1, width), routes.T, route_logits.T, w_gate, w_up, w_down)
 
 
 def solution(mesh):

time: 61.1 us -> 56.5 us (0.925)
  local copies, waits for them, and re-layouts: 4.29 us -> 1.57 us
  Pallas kernels: 56.6 us -> 54.8 us
    unnamed x3 -> x1, local copies, waits for them, and re-layouts: 4.29 us -> 1.57 us
    pallas_call x1, Pallas kernels: 56.6 us -> 54.8 us  [shards(): pl.pallas_call(functools.partial(layer, n, cap, zs, ys), out_shape=jax.Sh...]
where the time goes in v3:
time: 56.5 us; the launch traced here: 56.4 us
  Pallas kernels  54.8 us (97%)
  local copies, waits for them, and re-layouts  1.57 us (3%)
    pallas_call x1, Pallas kernels, shards(): pl.pallas_call(functools.partial(layer, n, cap, zs, ys), out_shape=jax.Sh...  54.8 us
    unnamed x1, local copies, waits for them, and re-layouts  1.57 us

profile of v3, /device:TPU:0, one launch (start us, length us, event | category | flops | bytes accessed | tf_op | source)
XLA Modules:
  0.0 56.4 jit_solution(288907788784970146)
XLA Ops:
  0.0 54.8 %shard_map.73 = bf16[32,2048]{1,0:T(8,128)(2,1)} custom-call(bf16[32,2048]{1,0:T(8,128)(2,1)} %x_ref.1, f32[1,2048]{1,0:T(1,128)} %bitcast.3, s32[4,32]{1,0:T(4,128)} %bitcast.4, f32[4,32]{1,0:T(4,128)} %bitcast.5, bf16[1,2048,1792]{2,1,0:T(8,128)(2,1)} %wg_hbm.1, bf16[1,2048,1792]{2,1,0:T(8,128)(2,1)} %wu_hbm.1, bf16[1,1792,2048]{2,1,0:T(8,128)(2,1)} %wd_hbm.1), custom_call_target="tpu_custom_call" | custom-call | tf_op jit(solution)/shard_map/pallas_call | solution.py:284
  54.8 1.6 %copy.9 = bf16[32,2048]{1,0:T(8,128)(2,1)} copy(bf16[32,2048]{1,0:T(8,128)(2,1)} %shard_map.73) | data formatting | bytes 262144

commit v4 on v3

--- a/solution.py
+++ b/solution.py
@@ -168,7 +168,7 @@
     for c in loads[:4]:
         c.wait()
 
-    @pl.loop(0, ff // TILE)
+    @pl.loop(0, ff // TILE, unroll=True)
     def _(t):
         cols = pl.ds(pl.multiple_of(t * TILE, TILE), TILE)
         gate = jnp.minimum(jnp.dot(X[...], wg[:, cols], preferred_element_type=F32), 7.0)
@@ -179,7 +179,7 @@
         c.wait()
 
     def down(base, dst):
-        @pl.loop(0, part // TILE)
+        @pl.loop(0, part // TILE, unroll=True)
         def _(t):
             cols = pl.ds(pl.multiple_of(base + t * TILE, TILE), TILE)
             here = pl.ds(pl.multiple_of(t * TILE, TILE), TILE)

time: 56.5 us -> 55.7 us (0.986)
  Pallas kernels: 54.8 us -> 54 us
    pallas_call x1, Pallas kernels: 54.8 us -> 54 us  [shards(): pl.pallas_call(functools.partial(layer, n, cap, zs, ys), out_shape=jax.Sh...]
where the time goes in v4:
time: 55.7 us; the launch traced here: 55.6 us
  Pallas kernels  54 us (97%)
  local copies, waits for them, and re-layouts  1.57 us (3%)
    pallas_call x1, Pallas kernels, shards(): pl.pallas_call(functools.partial(layer, n, cap, zs, ys), out_shape=jax.Sh...  54 us
    unnamed x1, local copies, waits for them, and re-layouts  1.57 us

profile of v4, /device:TPU:0, one launch (start us, length us, event | category | flops | bytes accessed | tf_op | source)
XLA Modules:
  0.0 55.6 jit_solution(10533025487310751178)
XLA Ops:
  0.0 54.0 %shard_map.73 = bf16[32,2048]{1,0:T(8,128)(2,1)} custom-call(bf16[32,2048]{1,0:T(8,128)(2,1)} %x_ref.1, f32[1,2048]{1,0:T(1,128)} %bitcast.3, s32[4,32]{1,0:T(4,128)} %bitcast.4, f32[4,32]{1,0:T(4,128)} %bitcast.5, bf16[1,2048,1792]{2,1,0:T(8,128)(2,1)} %wg_hbm.1, bf16[1,2048,1792]{2,1,0:T(8,128)(2,1)} %wu_hbm.1, bf16[1,1792,2048]{2,1,0:T(8,128)(2,1)} %wd_hbm.1), custom_call_target="tpu_custom_call" | custom-call | tf_op jit(solution)/shard_map/pallas_call | solution.py:284
  54.0 1.6 %copy.9 = bf16[32,2048]{1,0:T(8,128)(2,1)} copy(bf16[32,2048]{1,0:T(8,128)(2,1)} %shard_map.73) | data formatting | bytes 262144
